TPU v7x, 32 devices: a whole 2x2x4 slice. The times are simulated.
32 devices in a mesh: sp: 4 (over z), fs: 4 (over y, x), tp: 2 (over core).
Axes of the slice: x: 2, y: 2, z: 4, core: 2. Of those that a mesh axis runs over, the one named last changes fastest.
Arguments:
- tokens: bfloat16 [2048, 2048], P(('fs', 'sp'), 'tp'), parts along dimension 0, may hold values from -6 to 6
- norm_gain: float32 [2048], replicated, may hold values from 0.1 to 1.9
- w_recur_in: bfloat16 [2048, 1024], P(None, 'tp'), may hold values from -0.125 to 0.125
- conv_weight: float32 [4, 1024], P(None, 'tp'), may hold values from -3 to 3
- w_gate_decay: bfloat16 [16, 64, 64], P('tp'), may hold values from -0.75 to 0.75
- w_gate_input: bfloat16 [16, 64, 64], P('tp'), may hold values from -0.75 to 0.75
- decay_base: float32 [1024], P('tp'), may hold values from 0 to 0.01, as said below
- extra_decay: float32 [2048, 16], P(('fs', 'sp'), 'tp'), parts along dimension 0, may hold values from 0 to 1, as said below
- w_query: bfloat16 [2048, 1024], P(None, 'tp'), may hold values from -1 to 1
- w_key: bfloat16 [2048, 256], P(None, 'tp'), may hold values from -20 to 20
- w_value: bfloat16 [2048, 256], P(None, 'tp'), may hold values from -0.125 to 0.125
- mix_lambda: float32 [8], P('tp'), may hold values from 0.3 to 0.8
- head_gain: float32 [128], replicated, may hold values from 0.1 to 1.9
- w_out_recur: bfloat16 [1024, 2048], P('tp'), may hold values from -0.125 to 0.125
- w_out_attend: bfloat16 [1024, 2048], P('tp'), may hold values from -0.125 to 0.125
- out_gain: float32 [2048], replicated, may hold values from 0.1 to 1.9
Outputs:
- mixed: bfloat16 [2048, 2048], P(('fs', 'sp', 'tp')), parts along dimension 0
There are 4 independent parts, one for each index of `fs`. A program takes and returns all parts, laid end to end along the dimension named above; an argument that names none is the same for every part. Nothing has to cross between parts.
Inputs may be any that keep to these rules, and one draw needn't show every extreme that they name: `decay_base`: positive rates of each channel. `extra_decay`: non-negative added log-decays.
All inputs are finite; a program needn't handle non-finite values.
Results may differ from a plain program's by a relative error of at most 0.012.
The roundings to bfloat16 on the way count: a program that leaves them out, or rounds other values in their place, can miss the bound.
Values may be sent and summed in bfloat16 or wider, within the bound.
A program may use at most 128 MiB of HBM per device.

v0:
```python
import jax
import jax.numpy as jnp
from jax import lax
from jax.sharding import PartitionSpec as P

D = 2048
HEAD = 64
DV = 128
lru_rate = 8.0
norm_eps = 1e-06


def shifted(block, axis, distance):
    devices = range(lax.axis_size(axis))
    route = [(i - distance, i) for i in devices if i - distance in devices]
    return lax.ppermute(block, axis, route)


def prefix(part, axis, combine, identity):
    place = lax.axis_index(axis)
    gathered = jax.tree.map(lambda a: lax.all_gather(a, axis), part)
    state = jax.tree.map(lambda a, e: jnp.zeros_like(a) + jnp.asarray(e, a.dtype), part, identity)

    def one(lap, state):
        return combine(
            state, jax.tree.map(lambda a: lax.dynamic_index_in_dim(a, lap, 0, False), gathered)
        )

    return lax.fori_loop(0, place, one, state)


def chain(earlier, later):
    return (earlier[0] * later[0], later[0] * earlier[1] + later[1])


def body(
    tokens,
    norm_gain,
    w_recur_in,
    conv_weight,
    w_gate_decay,
    w_gate_input,
    decay_base,
    extra_decay,
    w_query,
    w_key,
    w_value,
    mix_lambda,
    head_gain,
    w_out_recur,
    w_out_attend,
    out_gain,
):
    row_count = tokens.shape[0]
    recur_cols = w_recur_in.shape[1]
    query_cols = w_query.shape[1]
    key_cols = w_key.shape[1]
    all_weights = jnp.concatenate([w_recur_in, w_query, w_key, w_value], axis=1)
    wide_piece = lax.all_gather(tokens, "tp", axis=1, tiled=True).astype(jnp.float32)
    scaled = (wide_piece * norm_gain).astype(jnp.bfloat16)
    accum = jnp.dot(scaled, all_weights, preferred_element_type=jnp.float32)
    squares = jnp.sum(wide_piece * wide_piece, axis=1, keepdims=True)
    accum, squares = (accum, squares)
    inverse = lax.rsqrt(squares / D + norm_eps)
    projected = (accum * inverse).astype(jnp.bfloat16)
    recur_in = projected[:, :recur_cols]
    queries = projected[:, recur_cols : recur_cols + query_cols]
    keys = projected[:, recur_cols + query_cols : recur_cols + query_cols + key_cols]
    values = projected[:, recur_cols + query_cols + key_cols :]
    taps = conv_weight.shape[0]
    carried_rows = shifted(recur_in[row_count - (taps - 1) :], "sp", 1)
    padded = jnp.concatenate([carried_rows, recur_in], axis=0).astype(jnp.float32)
    conv_acc = jnp.zeros((row_count, recur_cols), jnp.float32)
    for offset in range(taps):
        conv_acc = conv_acc + conv_weight[offset] * padded[offset : offset + row_count]
    conv_in = conv_acc.astype(jnp.bfloat16)
    gate_blocks = w_gate_decay.shape[0]
    blocks = conv_in.reshape(row_count, gate_blocks, HEAD)
    decay_gate = jax.nn.sigmoid(
        jnp.einsum("thi,hij->thj", blocks, w_gate_decay, preferred_element_type=jnp.float32)
    ).reshape(row_count, recur_cols)
    input_gate = jax.nn.sigmoid(
        jnp.einsum("thi,hij->thj", blocks, w_gate_input, preferred_element_type=jnp.float32)
    ).reshape(row_count, recur_cols)
    log_decay = -lru_rate * decay_gate * decay_base - jnp.repeat(extra_decay, HEAD, axis=1)
    decay = jnp.exp(log_decay)
    inject = jnp.sqrt(-jnp.expm1(2.0 * log_decay)) * input_gate * conv_in.astype(jnp.float32)
    decay_cum, local_state = lax.associative_scan(chain, (decay, inject), axis=0)
    identity = (jnp.ones((recur_cols,), jnp.float32), jnp.zeros((recur_cols,), jnp.float32))
    carried = prefix((decay_cum[row_count - 1], local_state[row_count - 1]), "sp", chain, identity)
    recur_out = (local_state + decay_cum * carried[1]).astype(jnp.bfloat16)
    kv_local = key_cols // (2 * HEAD)
    heads_local = query_cols // (2 * HEAD)
    group_size = heads_local // kv_local
    local_query = queries.reshape(row_count, kv_local, group_size, 2, HEAD)
    offset_rows = lax.axis_index("sp") * row_count
    positions = offset_rows + jnp.arange(row_count, dtype=jnp.int32)
    last_position = offset_rows + row_count - 1
    lambdas = mix_lambda.reshape(kv_local, group_size)
    start_state = (
        jnp.full((2, kv_local, group_size, row_count), -1e30, jnp.float32),
        jnp.zeros((2, kv_local, group_size, row_count), jnp.float32),
        jnp.zeros((2, row_count, kv_local, group_size, DV), jnp.float32),
    )
    key_piece = lax.all_gather(keys, "sp", axis=0, tiled=True)
    value_piece = lax.all_gather(values, "sp", axis=0, tiled=True)
    count = key_piece.shape[0]

    def update(state):
        peaks, totals, attends = state
        key_three = key_piece.reshape(count, kv_local, 2, HEAD)
        value_three = value_piece.reshape(count, kv_local, DV)
        allowed = positions[:, None] >= jnp.arange(count, dtype=jnp.int32)[None, :]
        new_peaks, new_totals, new_attends = ([], [], [])
        for mapping in range(2):
            scores = jnp.einsum(
                "bkgd,tkd->kgbt",
                local_query[:, :, :, mapping, :],
                key_three[:, :, mapping, :],
                preferred_element_type=jnp.float32,
            ) * HEAD ** (-0.5)
            scores = jnp.where(allowed, scores, -jnp.inf)
            peak = jnp.maximum(peaks[mapping], jnp.max(scores, axis=-1))
            correction = jnp.exp(peaks[mapping] - peak)
            expo = jnp.exp(scores - peak[..., None])
            new_totals.append(totals[mapping] * correction + jnp.sum(expo, axis=-1))
            gained = jnp.einsum(
                "kgbt,tke->bkge",
                expo.astype(jnp.bfloat16),
                value_three,
                preferred_element_type=jnp.float32,
            )
            new_attends.append(
                attends[mapping] * jnp.transpose(correction, (2, 0, 1))[..., None] + gained
            )
            new_peaks.append(peak)
        return (jnp.stack(new_peaks), jnp.stack(new_totals), jnp.stack(new_attends))

    peaks, totals, attends = lax.cond(
        jnp.int32(0) <= last_position, update, lambda state: state, start_state
    )
    first = attends[0] / jnp.transpose(totals[0], (2, 0, 1))[..., None]
    second = attends[1] / jnp.transpose(totals[1], (2, 0, 1))[..., None]
    head_out = (first - lambdas[None, :, :, None] * second).reshape(row_count, heads_local, DV)
    normed = (
        head_out
        * lax.rsqrt(jnp.mean(head_out * head_out, axis=-1, keepdims=True) + norm_eps)
        * head_gain
    )
    attend_out = normed.astype(jnp.bfloat16).reshape(row_count, heads_local * DV)
    recur_rows, attend_rows = (
        lax.all_to_all(recur_out, "tp", split_axis=0, concat_axis=1, tiled=True),
        lax.all_to_all(attend_out, "tp", split_axis=0, concat_axis=1, tiled=True),
    )
    whole_recur, whole_attend = (
        lax.all_gather(w_out_recur, "tp", axis=0, tiled=True),
        lax.all_gather(w_out_attend, "tp", axis=0, tiled=True),
    )
    merged = jnp.dot(recur_rows, whole_recur, preferred_element_type=jnp.float32) + jnp.dot(
        attend_rows, whole_attend, preferred_element_type=jnp.float32
    )
    final = (
        merged * lax.rsqrt(jnp.mean(merged * merged, axis=1, keepdims=True) + norm_eps) * out_gain
    )
    return final.astype(jnp.bfloat16)


def solution(mesh):
    in_specs = (
        P(("fs", "sp"), "tp"),
        P(),
        P(None, "tp"),
        P(None, "tp"),
        P("tp", None, None),
        P("tp", None, None),
        P("tp"),
        P(("fs", "sp"), "tp"),
        P(None, "tp"),
        P(None, "tp"),
        P(None, "tp"),
        P("tp"),
        P(),
        P("tp", None),
        P("tp", None),
        P(),
    )
    out_specs = P(("fs", "sp", "tp"), None)
    return jax.shard_map(body, mesh=mesh, in_specs=in_specs, out_specs=out_specs, check_vma=False)
```

profile of v0, /device:TPU:0, one launch (start us, length us, event | category | flops | bytes accessed | tf_op | source)
XLA Modules:
  0.0 101.6 jit_solution(12139623973826426824)
XLA Ops:
  6.5 0.7 all-gather.5.cloned.1.call-update
  7.3 2.5 %all_gather.21 = bf16[128,2048]{1,0:T(8,128)(2,1)S(1)} all-gather(bf16[128,1024]{1,0:T(8,128)(2,1)} %param.20), channel_id=1, replica_groups=mesh['sp'=4,'fs'=4,'tp'=2] {'tp'}, dimensions={1}, use_global_device_ids=true | all-gather | bytes 786432 | tf_op jit(solution)/shard_map/all_gather | solution.py:59
  10.0 3.2 %fusion.33 = bf16[128,1280]{1,0:T(8,128)(2,1)S(1)} fusion(bf16[2048,128]{1,0:T(8,128)(2,1)} %param.30, bf16[2048,128]{1,0:T(8,128)(2,1)} %param.29, bf16[2048,512]{1,0:T(8,128)(2,1)} %param.28, bf16[2048,512]{1,0:T(8,128)(2,1)} %param.22, bf16[128,2048]{1,0:T(8,128)(2,1)S(1)} %all_gather.21, f32[2048]{0:T(1024)} %param.21, f32[128]{0:T(128)S(1)} %add_rsqrt_fusion.2), kind=kOutput, calls=%fused_computation.52 | convolution fusion | flops 693174272 | bytes 6103552 | tf_op jit(solution)/shard_map/dot_general | solution.py:61
  13.2 4.8 %collective-permute-start = (bf16[3,512]{1,0:T(4,128)(2,1)S(1)}, bf16[3,512]{1,0:T(4,128)(2,1)S(1)}, u32[]{:S(2)}, u32[]{:S(2)}) collective-permute-start(bf16[3,512]{1,0:T(4,128)(2,1)S(1)} %slice.358), channel_id=1, source_target_pairs={{0,8},{8,16},{16,24},{1,9},{9,17},{17,25},{2,10},{10,18},{18,26},{... | collective-permute-start | bytes 9224 | tf_op jit(solution)/shard_map/ppermute | solution.py:16
  18.0 13.6 %all_gather.25 = bf16[512,128]{1,0:T(8,128)(2,1)S(1)} all-gather(bf16[128,128]{1,0:T(8,128)(2,1)S(1)} %get-tuple-element.115), channel_id=1, replica_groups=mesh['sp'=4,'fs'=4,'tp'=2] {'sp'}, dimensions={0}, use_global_device_ids=true | all-gather | bytes 163840 | tf_op jit(solution)/shard_map/all_gather | solution.py:105
  31.6 13.4 %all_gather.26 = bf16[512,128]{1,0:T(8,128)(2,1)S(1)} all-gather(bf16[128,128]{1,0:T(8,128)(2,1)S(1)} %get-tuple-element.114), channel_id=1, replica_groups=mesh['sp'=4,'fs'=4,'tp'=2] {'sp'}, dimensions={0}, use_global_device_ids=true | all-gather | bytes 163840 | tf_op jit(solution)/shard_map/all_gather | solution.py:106
  45.0 2.2 %conditional.1 = (f32[2,1,4,128]{3,2,1,0:T(4,128)S(1)}, f32[2,128,1,4,128]{4,1,3,2,0:T(8,128)S(1)}) conditional(s32[]{:T(128)} %convert_element_type.45, () %tuple.21, (s32[]{:T(128)}, s32[128]{0:T(128)S(1)}, bf16[512,128]{1,0:T(8,128)(2,1)S(1)}, bf16[128,1280]{1,0:T(8,128)(2,1)S(1)}, bf16[512,128]{1,0:T(8,128)(2,1)S(1)}) %tuple.22), branch_computations={%region_3.4_spmd, %region_4.9_spmd} | conditional | flops 205328512 | bytes 9819668 | solution.py:139
  45.4 0.3 fusion.65
  46.0 0.3 fusion.66
  46.5 0.4 fusion.5
  46.9 0.4 fusion.7
  47.5 0.3 fusion.53
  49.7 0.8 multiply_convert_fusion.1
  50.5 3.4 %all-to-all-start.1 = ((bf16[2,64,512]{2,1,0:T(8,128)(2,1)}), bf16[2,64,512]{2,1,0:T(8,128)(2,1)S(1)}, u32[]{:S(2)}, u32[]{:S(2)}) async-start(bf16[2,64,512]{2,1,0:T(8,128)(2,1)} %multiply_convert_fusion.1), calls=%async_computation.1 | async-start | bytes 262144 | tf_op jit(solution)/shard_map/all_to_all | solution.py:153
  53.9 0.7 all-gather.7.cloned.1.call-update
  54.8 0.5 all-to-all-done.1
  56.0 0.3 fusion.38
  56.5 0.3 convert_multiply_fusion.2
  59.6 11.9 %all-gather.1 = f32[4,1,512]{2,1,0:T(1,128)S(1)} all-gather(f32[1,1,512]{2,1,0:T(1,128)S(1)} %add_bitcast_fusion.2), channel_id=1, replica_groups=mesh['sp'=4,'fs'=4,'tp'=2] {'sp'}, dimensions={0}, use_global_device_ids=true | all-gather | bytes 10240 | tf_op jit(solution)/shard_map/all_gather | solution.py:21
  71.7 11.9 %all-gather = f32[4,1,512]{2,1,0:T(1,128)S(1)} all-gather(f32[1,1,512]{2,1,0:T(1,128)S(1)} %add_bitcast_fusion.3), channel_id=1, replica_groups=mesh['sp'=4,'fs'=4,'tp'=2] {'sp'}, dimensions={0}, use_global_device_ids=true | all-gather | bytes 10240 | tf_op jit(solution)/shard_map/all_gather | solution.py:21
  83.8 3.8 %all_to_all.35 = bf16[2,64,512]{2,1,0:T(8,128)(2,1)S(1)} all-to-all(bf16[2,64,512]{2,1,0:T(8,128)(2,1)S(1)} %bitcast.174), channel_id=1, replica_groups=mesh['sp'=4,'fs'=4,'tp'=2] {'tp'}, dimensions={0} | all-to-all | bytes 262144 | tf_op jit(solution)/shard_map/all_to_all | solution.py:152
  87.6 3.0 %fusion.71 = f32[64,2048]{1,0:T(8,128)S(1)} fusion(bf16[64,1024]{1,0:T(8,128)(2,1)S(1)} %bitcast.175, bf16[1024,2048]{1,0:T(8,128)(2,1)} %all-gather.5.cloned.1.call-done), kind=kOutput, calls=%fused_computation.154 | convolution fusion | flops 268435456 | bytes 4849664 | tf_op jit(solution)/shard_map/dot_general | solution.py:159
  90.7 3.2 %multiply_reduce_fusion = (f32[64]{0:T(128)S(1)}, f32[64,2048]{1,0:T(8,128)S(1)}) fusion(f32[64,2048]{1,0:T(8,128)S(1)} %fusion.71, bf16[64,1024]{1,0:T(8,128)(2,1)S(1)} %bitcast.173, bf16[1024,2048]{1,0:T(8,128)(2,1)} %all-gather.7.cloned.1.call-done), kind=kOutput, calls=%fused_computation.67 | convolution fusion | flops 268828608 | bytes 5374208 | tf_op jit(solution)/shard_map/dot_general | solution.py:159
  93.9 0.8 multiply_convert_fusion
  (179 shorter events, 6.6 us)
Async XLA Ops:
  6.5 49.1 %copy-start = (bf16[8,64,64]{2,1,0:T(8,128)(2,1)S(1)}, bf16[8,64,64]{2,1,0:T(8,128)(2,1)}, u32[]{:S(2)}) copy-start(bf16[8,64,64]{2,1,0:T(8,128)(2,1)} %param.24) | copy-start | bytes 196612
  6.5 81.1 %all-gather.5.cloned.1.call-start = ((), (), s32[]{:S(2)}) async-start(), calls=%async_computation.2 | async-start | bytes 6291456 | tf_op jit(solution)/shard_map/all_gather | solution.py:156
  13.2 42.1 %collective-permute-start = (bf16[3,512]{1,0:T(4,128)(2,1)S(1)}, bf16[3,512]{1,0:T(4,128)(2,1)S(1)}, u32[]{:S(2)}, u32[]{:S(2)}) collective-permute-start(bf16[3,512]{1,0:T(4,128)(2,1)S(1)} %slice.358), channel_id=1, source_target_pairs={{0,8},{8,16},{16,24},{1,9},{9,17},{17,25},{2,10},{10,18},{18,26},{... | collective-permute-start | bytes 9224 | tf_op jit(solution)/shard_map/ppermute | solution.py:16
  45.0 2.5 %copy-start.4 = (f32[4]{0:T(128)S(1)}, f32[4]{0:T(128)}, u32[]{:S(2)}) copy-start(f32[4]{0:T(128)} %param.31) | copy-start | bytes 52
  47.3 2.3 %copy-start.6 = (f32[128]{0:T(128)S(1)}, f32[128]{0:T(128)}, u32[]{:S(2)}) copy-start(f32[128]{0:T(128)} %param.32) | copy-start | bytes 1540
  48.3 6.3 %copy-start.2 = (f32[4,512]{1,0:T(4,128)S(1)}, f32[4,512]{1,0:T(4,128)}, u32[]{:S(2)}) copy-start(f32[4,512]{1,0:T(4,128)} %param.23) | copy-start | bytes 24580
  48.3 6.3 %copy-start.5 = (f32[512]{0:T(512)S(1)}, f32[512]{0:T(512)}, u32[]{:S(2)}) copy-start(f32[512]{0:T(512)} %param.26) | copy-start | bytes 6148
  48.4 6.3 %copy-start.3 = (f32[128,8]{0,1:T(8,128)S(1)}, f32[128,8]{0,1:T(8,128)}, u32[]{:S(2)}) copy-start(f32[128,8]{0,1:T(8,128)} %param.27) | copy-start | bytes 12292
  49.7 6.4 %copy-start.7 = (bf16[8,64,64]{2,1,0:T(8,128)(2,1)S(1)}, bf16[8,64,64]{2,1,0:T(8,128)(2,1)}, u32[]{:S(2)}) copy-start(bf16[8,64,64]{2,1,0:T(8,128)(2,1)} %param.25) | copy-start | bytes 196612
  50.5 4.8 %all-to-all-start.1 = ((bf16[2,64,512]{2,1,0:T(8,128)(2,1)}), bf16[2,64,512]{2,1,0:T(8,128)(2,1)S(1)}, u32[]{:S(2)}, u32[]{:S(2)}) async-start(bf16[2,64,512]{2,1,0:T(8,128)(2,1)} %multiply_convert_fusion.1), calls=%async_computation.1 | async-start | bytes 262144 | tf_op jit(solution)/shard_map/all_to_all | solution.py:153
  53.8 36.9 %all-gather.7.cloned.1.call-start = ((), (), s32[]{:S(2)}) async-start(), calls=%async_computation.3 | async-start | bytes 6291456 | tf_op jit(solution)/shard_map/all_gather | solution.py:157
  87.6 6.3 %copy-start.1 = (f32[2048]{0:T(1024)S(1)}, f32[2048]{0:T(1024)}, u32[]{:S(2)}) copy-start(f32[2048]{0:T(1024)} %param.35) | copy-start | bytes 24580
Sparse Core Ops, SparseCore 0:
  8.9 16.3 all-gather.4
  56.2 12.8 all-gather.6
where the time goes:
time: 102 us
  blocking collectives  57.2 us (56%)
  between operations  14.4 us (14%)
  matrix products  11.3 us (11%)
  starting transfers between devices  8.26 us (8%)
  local copies, waits for them, and re-layouts  4.75 us (5%)
  other arithmetic  3.69 us (4%)
  waiting for transfers between devices  1.91 us (2%)
    all_gather x2, blocking collectives, prefix(): gathered = jax.tree.map(lambda a: lax.all_gather(a, axis), part)  23.9 us
    all_gather x1, blocking collectives, body(): key_piece = lax.all_gather(keys, 'sp', axis=0, tiled=True)  13.6 us
    all_gather x1, blocking collectives, body(): value_piece = lax.all_gather(values, 'sp', axis=0, tiled=True)  13.4 us
    ppermute x1, starting transfers between devices, shifted(): return lax.ppermute(block, axis, route)  4.84 us
    all_to_all x1, blocking collectives, body(): lax.all_to_all(recur_out, 'tp', split_axis=0, concat_axis=1, tiled=True)  3.84 us
    all_to_all x1, starting transfers between devices, body(): lax.all_to_all(attend_out, 'tp', split_axis=0, concat_axis=1, tiled=True)  3.38 us
    dot_general x1, matrix products, body(): accum = jnp.dot(scaled, all_weights, preferred_element_type=jnp.float32)  3.19 us
    dot_general x1, matrix products, body(): jnp.dot(attend_rows, whole_attend, preferred_element_type=jnp.float32)  3.16 us
  transfers between devices with their start and end apart: 4, of which 1 were waited for; matrix products, arithmetic and copies ran while one was open for 15% of the time, Pallas kernels for 0%

commit v1 on v0

--- a/solution.py
+++ b/solution.py
@@ -103,7 +103,12 @@
         jnp.zeros((2, row_count, kv_local, group_size, DV), jnp.float32),
     )
     key_piece = lax.all_gather(keys, "sp", axis=0, tiled=True)
-    value_piece = lax.all_gather(values, "sp", axis=0, tiled=True)
+    ring = [values]
+    for hop in range(3):
+        ring.append(lax.ppermute(ring[-1], "sp", [(dev, (dev + 1) % 4) for dev in range(4)]))
+    value_piece = jnp.roll(
+        jnp.concatenate(ring[::-1], axis=0), (lax.axis_index("sp") + 1) * ring[0].shape[0], axis=0
+    )
     count = key_piece.shape[0]
 
     def update(state):

time: 102 us -> 97.9 us (0.960)
  blocking collectives: 57.2 us -> 48.3 us
  waiting for transfers between devices: 1.91 us -> 9.16 us
  starting transfers between devices: 8.26 us -> 6.55 us
    all_gather x1 -> x0, blocking collectives: 13.4 us -> none  [body(): value_piece = lax.all_gather(values, 'sp', axis=0, tiled=True)]
    ppermute x0 -> x3, waiting for transfers between devices: none -> 7.42 us  [body(): lax.ppermute(ring[-1], 'sp', [(dev, (dev + 1) % 4) for dev in range(4)])]
    all_to_all x0 -> x1, blocking collectives: none -> 3.84 us  [body(): lax.all_to_all(attend_out, 'tp', split_axis=0, concat_axis=1, tiled=True)]
    all_to_all x1 -> x0, starting transfers between devices: 3.38 us -> none  [body(): lax.all_to_all(attend_out, 'tp', split_axis=0, concat_axis=1, tiled=True)]
    ppermute x0 -> x3, starting transfers between devices: none -> 3.04 us  [body(): lax.ppermute(ring[-1], 'sp', [(dev, (dev + 1) % 4) for dev in range(4)])]
    ppermute x1, starting transfers between devices: 4.84 us -> 3.47 us  [shifted(): return lax.ppermute(block, axis, route)]
  transfers between devices with their start and end apart: 4 -> 6, of which waited for: 1 -> 3; matrix products, arithmetic and copies ran while one was open for 15% -> 15% of each run, Pallas kernels for 0% -> 0%
where the time goes in v1:
time: 97.9 us; the launch traced here: 97.6 us
  blocking collectives  48.3 us (49%)
  between operations  14.4 us (15%)
  matrix products  11.3 us (12%)
  waiting for transfers between devices  9.16 us (9%)
  starting transfers between devices  6.55 us (7%)
  local copies, waits for them, and re-layouts  4.94 us (5%)
  other arithmetic  2.85 us (3%)
    all_gather x2, blocking collectives, prefix(): gathered = jax.tree.map(lambda a: lax.all_gather(a, axis), part)  24.8 us
    all_gather x1, blocking collectives, body(): key_piece = lax.all_gather(keys, 'sp', axis=0, tiled=True)  13.3 us
    ppermute x3, waiting for transfers between devices, body(): lax.ppermute(ring[-1], 'sp', [(dev, (dev + 1) % 4) for dev in range(4)])  7.42 us
    all_to_all x1, blocking collectives, body(): lax.all_to_all(recur_out, 'tp', split_axis=0, concat_axis=1, tiled=True)  3.84 us
    all_to_all x1, blocking collectives, body(): lax.all_to_all(attend_out, 'tp', split_axis=0, concat_axis=1, tiled=True)  3.84 us
    ppermute x1, starting transfers between devices, shifted(): return lax.ppermute(block, axis, route)  3.47 us
    dot_general x1, matrix products, body(): accum = jnp.dot(scaled, all_weights, preferred_element_type=jnp.float32)  3.19 us
    dot_general x1, matrix products, body(): jnp.dot(attend_rows, whole_attend, preferred_element_type=jnp.float32)  3.16 us
  transfers between devices with their start and end apart: 6, of which 3 were waited for; matrix products, arithmetic and copies ran while one was open for 15% of the time, Pallas kernels for 0%

profile of v1, /device:TPU:0, one launch (start us, length us, event | category | flops | bytes accessed | tf_op | source)
XLA Modules:
  0.0 97.6 jit_solution(2115988486065965241)
XLA Ops:
  6.5 0.7 all-gather.5.cloned.1.call-update
  7.3 2.5 %all_gather.18 = bf16[128,2048]{1,0:T(8,128)(2,1)S(1)} all-gather(bf16[128,1024]{1,0:T(8,128)(2,1)} %param.20), channel_id=1, replica_groups=mesh['sp'=4,'fs'=4,'tp'=2] {'tp'}, dimensions={1}, use_global_device_ids=true | all-gather | bytes 786432 | tf_op jit(solution)/shard_map/all_gather | solution.py:59
  10.1 3.2 %fusion.37 = bf16[128,1280]{1,0:T(8,128)(2,1)S(1)} fusion(bf16[2048,128]{1,0:T(8,128)(2,1)} %param.30, bf16[2048,128]{1,0:T(8,128)(2,1)} %param.29, bf16[2048,512]{1,0:T(8,128)(2,1)} %param.28, bf16[2048,512]{1,0:T(8,128)(2,1)} %param.22, bf16[128,2048]{1,0:T(8,128)(2,1)S(1)} %all_gather.18, f32[2048]{0:T(1024)} %param.21, f32[128]{0:T(128)S(1)} %add_rsqrt_fusion.2), kind=kOutput, calls=%fused_computation.56 | convolution fusion | flops 693174272 | bytes 6103552 | tf_op jit(solution)/shard_map/dot_general | solution.py:61
  13.3 3.0 %collective-permute-start.1 = (bf16[128,128]{1,0:T(8,128)(2,1)S(1)}, bf16[128,128]{1,0:T(8,128)(2,1)S(1)}, u32[]{:S(2)}, u32[]{:S(2)}) collective-permute-start(bf16[128,128]{1,0:T(8,128)(2,1)S(1)} %slice.431), channel_id=1, source_target_pairs={{0,8},{8,16},{16,24},{24,0},{1,9},{9,17},{17,25},{25,1},{2,10},{10... | collective-permute-start | bytes 98312 | tf_op jit(solution)/shard_map/ppermute | solution.py:108
  16.3 3.5 %collective-permute-start = (bf16[3,512]{1,0:T(4,128)(2,1)S(1)}, bf16[3,512]{1,0:T(4,128)(2,1)S(1)}, u32[]{:S(2)}, u32[]{:S(2)}) collective-permute-start(bf16[3,512]{1,0:T(4,128)(2,1)S(1)} %slice.378), channel_id=1, source_target_pairs={{0,8},{8,16},{16,24},{1,9},{9,17},{17,25},{2,10},{10,18},{18,26},{... | collective-permute-start | bytes 9224 | tf_op jit(solution)/shard_map/ppermute | solution.py:16
  20.1 1.0 collective-permute-done
  21.4 0.3 fusion.45
  21.8 0.3 fusion.42
  22.2 0.3 convert_multiply_fusion.2
  25.5 12.9 %all-gather.1 = f32[4,1,512]{2,1,0:T(1,128)S(1)} all-gather(f32[1,1,512]{2,1,0:T(1,128)S(1)} %add_bitcast_fusion.2), channel_id=1, replica_groups=mesh['sp'=4,'fs'=4,'tp'=2] {'sp'}, dimensions={0}, use_global_device_ids=true | all-gather | bytes 10240 | tf_op jit(solution)/shard_map/all_gather | solution.py:21
  38.4 11.9 %all-gather = f32[4,1,512]{2,1,0:T(1,128)S(1)} all-gather(f32[1,1,512]{2,1,0:T(1,128)S(1)} %add_bitcast_fusion.3), channel_id=1, replica_groups=mesh['sp'=4,'fs'=4,'tp'=2] {'sp'}, dimensions={0}, use_global_device_ids=true | all-gather | bytes 10240 | tf_op jit(solution)/shard_map/all_gather | solution.py:21
  50.4 5.7 %collective-permute-done.2 = bf16[128,128]{1,0:T(8,128)(2,1)S(1)} collective-permute-done((bf16[128,128]{1,0:T(8,128)(2,1)S(1)}, bf16[128,128]{1,0:T(8,128)(2,1)S(1)}, u32[]{:S(2)}, u32[]{:S(2)}) %collective-permute-start.2) | collective-permute-done | bytes 32800 | tf_op jit(solution)/shard_map/ppermute | solution.py:108
  56.2 3.8 %all_to_all.35 = bf16[2,64,512]{2,1,0:T(8,128)(2,1)S(1)} all-to-all(bf16[2,64,512]{2,1,0:T(8,128)(2,1)S(1)} %bitcast.171), channel_id=1, replica_groups=mesh['sp'=4,'fs'=4,'tp'=2] {'tp'}, dimensions={0} | all-to-all | bytes 262144 | tf_op jit(solution)/shard_map/all_to_all | solution.py:157
  60.0 1.7 %collective-permute-done.3 = bf16[128,128]{1,0:T(8,128)(2,1)S(1)} collective-permute-done((bf16[128,128]{1,0:T(8,128)(2,1)S(1)}, bf16[128,128]{1,0:T(8,128)(2,1)S(1)}, u32[]{:S(2)}, u32[]{:S(2)}) %collective-permute-start.3) | collective-permute-done | bytes 32800 | tf_op jit(solution)/shard_map/ppermute | solution.py:108
  61.9 13.3 %all_gather.22 = bf16[512,128]{1,0:T(8,128)(2,1)S(1)} all-gather(bf16[128,128]{1,0:T(8,128)(2,1)S(1)} %get-tuple-element.246), channel_id=1, replica_groups=mesh['sp'=4,'fs'=4,'tp'=2] {'sp'}, dimensions={0}, use_global_device_ids=true | all-gather | bytes 163840 | tf_op jit(solution)/shard_map/all_gather | solution.py:105
  75.2 2.4 %conditional.1 = (f32[2,1,4,128]{3,2,1,0:T(4,128)S(1)}, f32[2,128,1,4,128]{1,4,3,2,0:T(8,128)S(1)}) conditional(s32[]{:T(128)} %convert_element_type.51, () %tuple.32, (s32[]{:T(128)}, s32[128]{0:T(128)S(1)}, bf16[512,128]{1,0:T(8,128)(2,1)S(1)}, bf16[128,1280]{1,0:T(8,128)(2,1)S(1)}, s32[]{:T(128)}, /*index=5*/s32[]{:T(128)}, ...), branch_computations={%region_3.4_spmd, %region_4.9_spmd.clone} | conditional | flops 205328512 | bytes 10344119 | solution.py:144
  75.7 0.3 fusion.69
  76.2 0.3 fusion.70
  76.9 0.3 fusion.5
  77.2 0.3 fusion.7
  79.8 3.8 %all_to_all.36 = bf16[2,64,512]{2,1,0:T(8,128)(2,1)S(1)} all-to-all(bf16[2,64,512]{2,1,0:T(8,128)(2,1)S(1)} %multiply_convert_fusion.1), channel_id=1, replica_groups=mesh['sp'=4,'fs'=4,'tp'=2] {'tp'}, dimensions={0} | all-to-all | bytes 262144 | tf_op jit(solution)/shard_map/all_to_all | solution.py:158
  83.7 3.0 %fusion.74 = f32[64,2048]{1,0:T(8,128)S(1)} fusion(bf16[64,1024]{1,0:T(8,128)(2,1)S(1)} %bitcast.169, bf16[1024,2048]{1,0:T(8,128)(2,1)} %all-gather.5.cloned.1.call-done), kind=kOutput, calls=%fused_computation.165 | convolution fusion | flops 268435456 | bytes 4849664 | tf_op jit(solution)/shard_map/dot_general | solution.py:164
  86.7 3.2 %multiply_reduce_fusion = (f32[64]{0:T(128)S(1)}, f32[64,2048]{1,0:T(8,128)S(1)}) fusion(f32[64,2048]{1,0:T(8,128)S(1)} %fusion.74, bf16[64,1024]{1,0:T(8,128)(2,1)S(1)} %bitcast.170, bf16[1024,2048]{1,0:T(8,128)(2,1)} %all-gather.7.cloned.1.call-done), kind=kOutput, calls=%fused_computation.71 | convolution fusion | flops 268828608 | bytes 5374208 | tf_op jit(solution)/shard_map/dot_general | solution.py:164
  89.9 0.8 multiply_convert_fusion
  (192 shorter events, 6.8 us)
Async XLA Ops:
  6.5 14.8 %copy-start = (bf16[8,64,64]{2,1,0:T(8,128)(2,1)S(1)}, bf16[8,64,64]{2,1,0:T(8,128)(2,1)}, u32[]{:S(2)}) copy-start(bf16[8,64,64]{2,1,0:T(8,128)(2,1)} %param.24) | copy-start | bytes 196612
  6.5 77.1 %all-gather.5.cloned.1.call-start = ((), (), s32[]{:S(2)}) async-start(), calls=%async_computation.2 | async-start | bytes 6291456 | tf_op jit(solution)/shard_map/all_gather | solution.py:161
  7.3 79.5 %all-gather.7.cloned.1.call-start = ((), (), s32[]{:S(2)}) async-start(), calls=%async_computation.3 | async-start | bytes 6291456 | tf_op jit(solution)/shard_map/all_gather | solution.py:162
  10.0 9.8 %copy-start.2 = (f32[4,512]{1,0:T(4,128)S(1)}, f32[4,512]{1,0:T(4,128)}, u32[]{:S(2)}) copy-start(f32[4,512]{1,0:T(4,128)} %param.23) | copy-start | bytes 24580
  10.0 9.8 %copy-start.4 = (f32[4]{0:T(128)S(1)}, f32[4]{0:T(128)}, u32[]{:S(2)}) copy-start(f32[4]{0:T(128)} %param.31) | copy-start | bytes 52
  10.0 9.8 %copy-start.6 = (f32[128]{0:T(128)S(1)}, f32[128]{0:T(128)}, u32[]{:S(2)}) copy-start(f32[128]{0:T(128)} %param.32) | copy-start | bytes 1540
  10.0 9.9 %copy-start.5 = (f32[512]{0:T(512)S(1)}, f32[512]{0:T(512)}, u32[]{:S(2)}) copy-start(f32[512]{0:T(512)} %param.26) | copy-start | bytes 6148
  10.1 9.9 %copy-start.3 = (f32[128,8]{0,1:T(8,128)S(1)}, f32[128,8]{0,1:T(8,128)}, u32[]{:S(2)}) copy-start(f32[128,8]{0,1:T(8,128)} %param.27) | copy-start | bytes 12292
  13.3 8.5 %copy-start.7 = (bf16[8,64,64]{2,1,0:T(8,128)(2,1)S(1)}, bf16[8,64,64]{2,1,0:T(8,128)(2,1)}, u32[]{:S(2)}) copy-start(bf16[8,64,64]{2,1,0:T(8,128)(2,1)} %param.25) | copy-start | bytes 196612
  13.3 37.0 %collective-permute-start.1 = (bf16[128,128]{1,0:T(8,128)(2,1)S(1)}, bf16[128,128]{1,0:T(8,128)(2,1)S(1)}, u32[]{:S(2)}, u32[]{:S(2)}) collective-permute-start(bf16[128,128]{1,0:T(8,128)(2,1)S(1)} %slice.431), channel_id=1, source_target_pairs={{0,8},{8,16},{16,24},{24,0},{1,9},{9,17},{17,25},{25,1},{2,10},{10... | collective-permute-start | bytes 98312 | tf_op jit(solution)/shard_map/ppermute | solution.py:108
  16.3 4.8 %collective-permute-start = (bf16[3,512]{1,0:T(4,128)(2,1)S(1)}, bf16[3,512]{1,0:T(4,128)(2,1)S(1)}, u32[]{:S(2)}, u32[]{:S(2)}) collective-permute-start(bf16[3,512]{1,0:T(4,128)(2,1)S(1)} %slice.378), channel_id=1, source_target_pairs={{0,8},{8,16},{16,24},{1,9},{9,17},{17,25},{2,10},{10,18},{18,26},{... | collective-permute-start | bytes 9224 | tf_op jit(solution)/shard_map/ppermute | solution.py:16
  50.3 5.8 %collective-permute-start.2 = (bf16[128,128]{1,0:T(8,128)(2,1)S(1)}, bf16[128,128]{1,0:T(8,128)(2,1)S(1)}, u32[]{:S(2)}, u32[]{:S(2)}) collective-permute-start(bf16[128,128]{1,0:T(8,128)(2,1)S(1)} %collective-permute-done.1), channel_id=1, source_target_pairs={{0,8},{8,16},{16,24},{24,0},{1,9},{9,17},{17,25},{25,1},{2,10},{10... | collective-permute-start | bytes 98312 | tf_op jit(solution)/shard_map/ppermute | solution.py:108
  56.1 5.7 %collective-permute-start.3 = (bf16[128,128]{1,0:T(8,128)(2,1)S(1)}, bf16[128,128]{1,0:T(8,128)(2,1)S(1)}, u32[]{:S(2)}, u32[]{:S(2)}) collective-permute-start(bf16[128,128]{1,0:T(8,128)(2,1)S(1)} %collective-permute-done.2), channel_id=1, source_target_pairs={{0,8},{8,16},{16,24},{24,0},{1,9},{9,17},{17,25},{25,1},{2,10},{10... | collective-permute-start | bytes 98312 | tf_op jit(solution)/shard_map/ppermute | solution.py:108
  83.7 6.3 %copy-start.1 = (f32[2048]{0:T(1024)S(1)}, f32[2048]{0:T(1024)}, u32[]{:S(2)}) copy-start(f32[2048]{0:T(1024)} %param.35) | copy-start | bytes 24580
Sparse Core Ops, SparseCore 0:
  8.9 16.3 all-gather.4
  26.8 14.8 all-gather.6
